TPU v7x, 32 devices: a whole 2x2x4 slice. The times are simulated.
32 devices in a mesh: fs: 8 (over z, y), tp: 4 (over x, core).
Axes of the slice: x: 2, y: 2, z: 4, core: 2. Of those that a mesh axis runs over, the one named last changes fastest.
Arguments:
- hidden_in: bfloat16 [512, 4096], P(None, 'tp'), may hold values from -6 to 6
- up_act: bfloat16 [512, 12288], P('tp', 'fs'), may hold values from -6 to 6
- up_val: bfloat16 [512, 12288], P('tp', 'fs'), may hold values from -6 to 6
- cotangent: bfloat16 [512, 4096], P('tp'), may hold values from -6 to 6
- w_act: bfloat16 [4096, 12288], P('tp', 'fs'), may hold values from -0.09375 to 0.09375
- w_val: bfloat16 [4096, 12288], P('tp', 'fs'), may hold values from -0.09375 to 0.09375
- w_down: bfloat16 [12288, 4096], P('fs', 'tp'), may hold values from -0.0546875 to 0.0546875
- conv_act: bfloat16 [3, 12288], P(None, 'fs'), may hold values from -3 to 3
- conv_val: bfloat16 [3, 12288], P(None, 'fs'), may hold values from -3 to 3
- bias_act: bfloat16 [12288], P('fs'), may hold values from -3 to 3
- bias_val: bfloat16 [12288], P('fs'), may hold values from -3 to 3
Outputs:
- grad_input: bfloat16 [512, 4096], P(('tp', 'fs'))
- grad_w_act: float32 [4096, 12288], P('tp', 'fs')
- grad_w_val: float32 [4096, 12288], P('tp', 'fs')
- grad_w_down: float32 [12288, 4096], P('fs', 'tp')
- grad_conv_act: float32 [3, 12288], P(None, 'fs')
- grad_conv_val: float32 [3, 12288], P(None, 'fs')
- grad_bias_act: float32 [12288], P('fs')
- grad_bias_val: float32 [12288], P('fs')
- rows_act: float32 [4096], P('tp')
- rows_val: float32 [4096], P('tp')
- rows_down: float32 [12288], P('fs')
- conv_rows: float32 [2, 3], replicated
All inputs are finite; a program needn't handle non-finite values.
Results may differ from a plain program's by a relative error of at most 0.0057.
Values may be sent and summed in bfloat16 or wider, within the bound.
A program may use at most 128 MiB of HBM per device.

v0:
```python
import jax
import jax.numpy as jnp
from jax import lax
from jax.sharding import PartitionSpec as P


def passed_along(value, axis, by):
    length = lax.axis_size(axis)
    pairs = [(i, i + by) for i in range(length) if 0 <= i + by < length]
    return lax.ppermute(value, axis, pairs)


def contract_last(left, right):
    return lax.dot_general(
        left, right, (((1,), (1,)), ((), ())), preferred_element_type=jnp.float32
    )


def contract_first(left, right):
    return lax.dot_general(
        left, right, (((0,), (0,)), ((), ())), preferred_element_type=jnp.float32
    )


def conv_ahead(extended, taps, bias, length):
    total = jnp.zeros((length, extended.shape[1]), jnp.float32) + bias.astype(jnp.float32)
    for offset in range(taps.shape[0]):
        total = total + taps[offset].astype(jnp.float32) * extended[offset : offset + length]
    return total


def conv_behind(extended, taps, length):
    reach = taps.shape[0] - 1
    total = jnp.zeros((length, extended.shape[1]), jnp.float32)
    for offset in range(taps.shape[0]):
        total = (
            total
            + taps[offset].astype(jnp.float32) * extended[reach - offset : reach - offset + length]
        )
    return total.astype(jnp.bfloat16)


def tap_grads(grad_pre, extended, tap_count):
    length = grad_pre.shape[0]
    rows = [
        jnp.sum(grad_pre * extended[offset : offset + length], axis=0)
        for offset in range(tap_count)
    ]
    return (jnp.stack(rows, 0), jnp.sum(grad_pre, axis=0))


def per_device(
    hidden_in,
    up_act,
    up_val,
    cotangent,
    w_act,
    w_val,
    w_down,
    conv_act,
    conv_val,
    bias_act,
    bias_val,
):
    local_rows = cotangent.shape[0]
    tap_count = conv_act.shape[0]
    reach = tap_count - 1
    tp_count = lax.axis_size("tp")
    fs_count = lax.axis_size("fs")
    down_whole = lax.all_gather(w_down, "tp", axis=1, tiled=True)
    prev_act, prev_val = passed_along(
        (up_act[local_rows - reach :], up_val[local_rows - reach :]), "tp", 1
    )
    ext_act = jnp.concatenate([prev_act, up_act], 0).astype(jnp.float32)
    ext_val = jnp.concatenate([prev_val, up_val], 0).astype(jnp.float32)
    pre_act = conv_ahead(ext_act, conv_act, bias_act, local_rows)
    pre_val = conv_ahead(ext_val, conv_val, bias_val, local_rows)
    gelu_act, gelu_back = jax.vjp(jax.nn.gelu, pre_act)
    mixed = (gelu_act * pre_val).astype(jnp.bfloat16)
    grad_mixed = contract_last(cotangent, down_whole).astype(jnp.bfloat16)
    grad_mixed = lax.optimization_barrier(grad_mixed).astype(jnp.float32)
    grad_pre_act = gelu_back(grad_mixed * pre_val)[0]
    grad_pre_val = grad_mixed * gelu_act
    next_act, next_val = passed_along((grad_pre_act[:reach], grad_pre_val[:reach]), "tp", -1)
    grad_up_act = conv_behind(jnp.concatenate([grad_pre_act, next_act], 0), conv_act, local_rows)
    grad_up_val = conv_behind(jnp.concatenate([grad_pre_val, next_val], 0), conv_val, local_rows)
    taps_act, sums_act = tap_grads(grad_pre_act, ext_act, tap_count)
    taps_val, sums_val = tap_grads(grad_pre_val, ext_val, tap_count)
    all_up_act, all_up_val, all_mixed = (
        lax.all_gather(grad_up_act, "tp", axis=0, tiled=True),
        lax.all_gather(grad_up_val, "tp", axis=0, tiled=True),
        lax.all_gather(mixed, "tp", axis=0, tiled=True),
    )
    cot_columns = lax.all_to_all(cotangent, "tp", split_axis=1, concat_axis=0, tiled=True)
    grad_w_act = contract_first(hidden_in, all_up_act)
    grad_w_val = contract_first(hidden_in, all_up_val)
    grad_w_down = contract_first(all_mixed, cot_columns)
    shard_rows = local_rows // fs_count
    block_rows = tp_count * shard_rows

    def select_rows(gathered):
        shaped = gathered.reshape(tp_count, fs_count, shard_rows, gathered.shape[1])
        return jnp.transpose(shaped, (1, 0, 2, 3)).reshape(
            lax.axis_size("fs") * block_rows, gathered.shape[1]
        )

    summed = lax.psum_scatter(
        contract_last(select_rows(all_up_act), w_act)
        + contract_last(select_rows(all_up_val), w_val),
        "fs",
        scatter_dimension=0,
        tiled=True,
    ).astype(jnp.bfloat16)
    grad_input = lax.all_to_all(summed, "tp", split_axis=0, concat_axis=1, tiled=True)
    down_squares = jnp.sum(grad_w_down * grad_w_down, axis=1)
    taps_act, taps_val, sums_act, sums_val, rows_down = lax.psum(
        (taps_act, taps_val, sums_act, sums_val, down_squares), "tp"
    )
    tap_squares = jnp.stack(
        [jnp.sum(taps_act * taps_act, axis=1), jnp.sum(taps_val * taps_val, axis=1)], 0
    )
    rows_act, rows_val, conv_rows = lax.psum(
        (
            jnp.sum(grad_w_act * grad_w_act, axis=1),
            jnp.sum(grad_w_val * grad_w_val, axis=1),
            tap_squares,
        ),
        "fs",
    )
    return (
        grad_input,
        grad_w_act,
        grad_w_val,
        grad_w_down,
        taps_act,
        taps_val,
        sums_act,
        sums_val,
        rows_act,
        rows_val,
        rows_down,
        conv_rows,
    )


def solution(mesh):
    return jax.shard_map(
        per_device,
        mesh=mesh,
        in_specs=(
            P(None, "tp"),
            P("tp", "fs"),
            P("tp", "fs"),
            P("tp", None),
            P("tp", "fs"),
            P("tp", "fs"),
            P("fs", "tp"),
            P(None, "fs"),
            P(None, "fs"),
            P("fs"),
            P("fs"),
        ),
        out_specs=(
            P(("tp", "fs"), None),
            P("tp", "fs"),
            P("tp", "fs"),
            P("fs", "tp"),
            P(None, "fs"),
            P(None, "fs"),
            P("fs"),
            P("fs"),
            P("tp"),
            P("tp"),
            P("fs"),
            P(),
        ),
        check_vma=False,
    )
```

profile of v0, /device:TPU:0, one launch (start us, length us, event | category | flops | bytes accessed | tf_op | source)
XLA Modules:
  0.0 296.1 jit_solution(9692622403794457745)
XLA Ops:
  8.4 2.4 collective-permute-start.1
  11.5 4.5 %collective-permute-start = (bf16[2,1536]{1,0:T(2,128)(2,1)S(1)}, bf16[2,1536]{1,0:T(2,128)(2,1)S(1)}, u32[]{:S(2)}, u32[]{:S(2)}) collective-permute-start(bf16[2,1536]{1,0:T(2,128)(2,1)S(1)} %slice.74), channel_id=1, source_target_pairs={{0,1},{1,2},{2,3},{4,5},{5,6},{6,7},{8,9},{9,10},{10,11},{12,13},{... | collective-permute-start | bytes 18440 | tf_op jit(solution)/shard_map/ppermute | solution.py:10
  16.0 1.5 convert_reduce_fusion.5
  17.5 1.3 convert_element_type.52
  19.8 2.1 maximum_convert_fusion
  21.9 72.5 %all-gather.5.cloned.1.call-done = bf16[1536,4096]{1,0:T(8,128)(2,1)} async-done(((bf16[1536,1024]{1,0:T(8,128)(2,1)}), bf16[1536,4096]{1,0:T(8,128)(2,1)}) %all-gather.5.cloned.1.call-update) | async-done | bytes 12582928 | tf_op jit(solution)/shard_map/all_gather | solution.py:70
  94.4 9.3 %convolution_convert_fusion = bf16[128,1536]{1,0:T(8,128)(2,1)S(1)} fusion(bf16[128,4096]{1,0:T(8,128)(2,1)} %param.14, bf16[1536,4096]{1,0:T(8,128)(2,1)} %all-gather.5.cloned.1.call-done), kind=kOutput, calls=%fused_computation.5 | convolution fusion | flops 1610809344 | bytes 14024704 | tf_op jit(solution)/shard_map/dot_general | solution.py:14
  104.7 1.3 collective-permute-start.3
  106.1 1.7 collective-permute-done.3
  107.8 2.1 multiply_reduce_fusion.8
  112.1 3.5 %collective-permute-done.2 = f32[2,1536]{1,0:T(2,128)S(1)} collective-permute-done((f32[2,1536]{1,0:T(2,128)S(1)}, f32[2,1536]{1,0:T(2,128)S(1)}, u32[]{:S(2)}, u32[]{:S(2)}) %collective-permute-start.2) | collective-permute-done | bytes 12320 | tf_op jit(solution)/shard_map/ppermute | solution.py:10
  115.5 3.0 fusion.9
  118.6 2.5 multiply_convert_fusion
  121.2 10.4 %all-gather.9.cloned.1.call-done = bf16[512,1536]{1,0:T(8,128)(2,1)} async-done(((bf16[128,1536]{1,0:T(8,128)(2,1)}), bf16[512,1536]{1,0:T(8,128)(2,1)}) %all-gather.9.cloned.1.call-update) | async-done | bytes 1572880 | tf_op jit(solution)/shard_map/all_gather | solution.py:91
  131.5 2.7 copy.34
  134.2 18.6 %all-gather.7.cloned.1.call-done = bf16[512,1536]{1,0:T(8,128)(2,1)} async-done(((bf16[128,1536]{1,0:T(8,128)(2,1)}), bf16[512,1536]{1,0:T(8,128)(2,1)}) %all-gather.7.cloned.1.call-update) | async-done | bytes 1572880 | tf_op jit(solution)/shard_map/all_gather | solution.py:90
  152.8 1.5 copy.33
  154.3 1.8 fusion.19
  156.7 3.2 %convolution_add_fusion = f32[512,1024]{1,0:T(8,128)} fusion(f32[512,1024]{1,0:T(8,128)S(1)} %fusion.19, bf16[512,1536]{1,0:T(8,128)(2,1)S(1)} %bitcast.37, bf16[1024,1536]{1,0:T(8,128)(2,1)S(1)} %copy-done.17), kind=kOutput, calls=%fused_computation.6 | convolution fusion | flops 1611137024 | bytes 8912896 | tf_op jit(solution)/shard_map/dot_general | solution.py:14
  161.8 21.8 %all_to_all.38 = bf16[128,4,1024]{0,2,1:T(8,128)(2,1)S(1)} all-to-all(bf16[128,4,1024]{0,2,1:T(8,128)(2,1)S(1)} %bitcast.34), channel_id=1, replica_groups=mesh['fs'=8,'tp'=4] {'tp'}, dimensions={1} | all-to-all | bytes 2097152 | tf_op jit(solution)/shard_map/all_to_all | solution.py:94
  183.6 1.3 copy.37
  185.4 5.8 %multiply_reduce_fusion.1 = (f32[1024]{0:T(1024)S(1)}, f32[1024,1536]{0,1:T(8,128)}) fusion(bf16[512,1536]{1,0:T(8,128)(2,1)S(1)} %copy-done.7, bf16[512,1024]{1,0:T(8,128)(2,1)} %param.11), kind=kOutput, calls=%fused_computation.1 | convolution fusion | flops 1613757440 | bytes 8916992 | tf_op jit(solution)/shard_map/dot_general | solution.py:20
  191.1 6.7 %copy.39 = f32[1024,1536]{1,0:T(8,128)} copy(f32[1024,1536]{0,1:T(8,128)} %get-tuple-element.80) | data formatting | bytes 12582912
  197.8 6.0 %multiply_reduce_fusion = (f32[1536]{0:T(1024)S(1)}, f32[1536,1024]{0,1:T(8,128)}) fusion(bf16[512,1536]{1,0:T(8,128)(2,1)} %all-gather.11.cloned.1.call-done, bf16[512,1024]{1,0:T(8,128)(2,1)S(1)} %bitcast.39), kind=kOutput, calls=%fused_computation | convolution fusion | flops 1613756928 | bytes 8919040 | tf_op jit(solution)/shard_map/dot_general | solution.py:20
  203.8 6.7 %copy.40 = f32[1536,1024]{1,0:T(8,128)} copy(f32[1536,1024]{0,1:T(8,128)} %get-tuple-element.76) | data formatting | bytes 12582912
  210.5 11.9 %all-reduce.1 = (f32[3,1536]{1,0:T(4,128)S(1)}, f32[3,1536]{1,0:T(4,128)S(1)}, f32[1536]{0:T(1024)}, f32[1536]{0:T(1024)}, f32[1536]{0:T(1024)}) all-reduce(f32[3,1536]{1,0:T(4,128)S(1)} %pad_maximum_fusion.2, f32[3,1536]{1,0:T(4,128)S(1)} %pad_maximum_fusion.3, ...), channel_id=1, replica_groups=mesh['fs'=8,'tp'=4] {'tp'}, use_global_device_ids=true, to_apply=%region_4.0 | all-reduce | flops 13824 | bytes 110592 | tf_op jit(solution)/shard_map/psum | solution.py:116
  222.6 28.7 %reduce-scatter.2.cloned.1.call-done = f32[64,1024]{1,0:T(8,128)} async-done(((f32[512,1024]{1,0:T(8,128)}), f32[64,1024]{1,0:T(8,128)}) %reduce-scatter.2.cloned.1.call-update) | async-done | bytes 262160 | tf_op jit(solution)/shard_map/reduce_scatter | solution.py:107
  251.3 1.6 convert_element_type.56
  252.9 3.3 %all-to-all-start = ((bf16[4,16,1024]{2,1,0:T(8,128)(2,1)}), bf16[4,16,1024]{2,1,0:T(8,128)(2,1)S(1)}, u32[]{:S(2)}, u32[]{:S(2)}) async-start(bf16[4,16,1024]{2,1,0:T(8,128)(2,1)} %bitcast.6), calls=%async_computation.1 | async-start | bytes 262144 | tf_op jit(solution)/shard_map/all_to_all | solution.py:114
  256.3 5.7 %multiply_reduce_fusion.2 = (f32[1024]{0:T(1024)S(1)}, f32[1024,1536]{0,1:T(8,128)}) fusion(bf16[512,1536]{1,0:T(8,128)(2,1)S(1)} %copy-done.6, bf16[512,1024]{1,0:T(8,128)(2,1)} %param.11), kind=kOutput, calls=%fused_computation.2 | convolution fusion | flops 1613757440 | bytes 8916992 | tf_op jit(solution)/shard_map/dot_general | solution.py:20
  262.0 6.7 %copy.38 = f32[1024,1536]{1,0:T(8,128)} copy(f32[1024,1536]{0,1:T(8,128)} %get-tuple-element.78) | data formatting | bytes 12582912
  268.7 20.2 %all-reduce = (f32[1024]{0:T(1024)}, f32[1024]{0:T(1024)}, f32[2,3]{1,0:T(2,128)}) all-reduce(f32[1024]{0:T(1024)S(1)} %get-tuple-element.77, f32[1024]{0:T(1024)S(1)} %get-tuple-element.79, f32[2,3]{1,0:T(2,128)S(1)} %pad_maximum_fusion.4), channel_id=1, replica_groups=mesh['fs'=8,'tp'=4] {'fs'}, use_global_device_ids=true, to_apply=%region_14.0 | all-reduce | flops 2054 | bytes 16432 | tf_op jit(solution)/shard_map/psum | solution.py:122
  (71 shorter events, 9.9 us)
Async XLA Ops:
  7.2 147.1 %copy-start = (bf16[1024,1536]{1,0:T(8,128)(2,1)S(1)}, bf16[1024,1536]{1,0:T(8,128)(2,1)}, u32[]{:S(2)}) copy-start(bf16[1024,1536]{1,0:T(8,128)(2,1)} %param.15) | copy-start | bytes 9437188
  7.2 1.1 copy-start.10
  7.2 87.2 %all-gather.5.cloned.1.call-start = ((), (), s32[]{:S(2)}) async-start(), calls=%async_computation.3 | async-start | bytes 15728640 | tf_op jit(solution)/shard_map/all_gather | solution.py:70
  7.9 123.6 %all-gather.9.cloned.1.call-start = ((), (), s32[]{:S(2)}) async-start(), calls=%async_computation.5 | async-start | bytes 1966080 | tf_op jit(solution)/shard_map/all_gather | solution.py:91
  8.4 10.4 %collective-permute-start.1 = (bf16[2,1536]{1,0:T(2,128)(2,1)S(1)}, bf16[2,1536]{1,0:T(2,128)(2,1)S(1)}, u32[]{:S(2)}, u32[]{:S(2)}) collective-permute-start(bf16[2,1536]{1,0:T(2,128)(2,1)S(1)} %slice.80), channel_id=1, source_target_pairs={{0,1},{1,2},{2,3},{4,5},{5,6},{6,7},{8,9},{9,10},{10,11},{12,13},{... | collective-permute-start | bytes 18440 | tf_op jit(solution)/shard_map/ppermute | solution.py:10
  11.5 8.3 %collective-permute-start = (bf16[2,1536]{1,0:T(2,128)(2,1)S(1)}, bf16[2,1536]{1,0:T(2,128)(2,1)S(1)}, u32[]{:S(2)}, u32[]{:S(2)}) collective-permute-start(bf16[2,1536]{1,0:T(2,128)(2,1)S(1)} %slice.74), channel_id=1, source_target_pairs={{0,1},{1,2},{2,3},{4,5},{5,6},{6,7},{8,9},{9,10},{10,11},{12,13},{... | collective-permute-start | bytes 18440 | tf_op jit(solution)/shard_map/ppermute | solution.py:10
  21.9 81.8 %copy-start.11 = (f32[1536]{0:T(1024)S(1)}, f32[1536]{0:T(1024)}, u32[]{:S(2)}) copy-start(f32[1536]{0:T(1024)} %get-tuple-element.61) | copy-start | bytes 18436
  21.9 81.8 %copy-start.12 = (f32[1536]{0:T(1024)S(1)}, f32[1536]{0:T(1024)}, u32[]{:S(2)}) copy-start(f32[1536]{0:T(1024)} %convert_element_type.52) | copy-start | bytes 18436
  94.4 9.3 %copy-start.2 = (f32[130,1536]{1,0:T(8,128)S(1)}, f32[130,1536]{1,0:T(8,128)}, u32[]{:S(2)}) copy-start(f32[130,1536]{1,0:T(8,128)} %maximum_convert_fusion.1) | copy-start | bytes 2396164
  94.4 9.3 %copy-start.3 = (f32[130,1536]{1,0:T(8,128)S(1)}, f32[130,1536]{1,0:T(8,128)}, u32[]{:S(2)}) copy-start(f32[130,1536]{1,0:T(8,128)} %maximum_convert_fusion) | copy-start | bytes 2396164
  103.8 2.2 copy-start.13
  103.8 2.3 copy-start.16
  104.7 5.2 %copy-start.4 = (f32[128,1536]{1,0:T(8,128)}, f32[128,1536]{1,0:T(8,128)S(1)}, u32[]{:S(2)}) copy-start(f32[128,1536]{1,0:T(8,128)S(1)} %get-tuple-element.71) | copy-start | bytes 2359300
  104.7 3.1 %collective-permute-start.3 = (f32[2,1536]{1,0:T(2,128)S(1)}, f32[2,1536]{1,0:T(2,128)S(1)}, u32[]{:S(2)}, u32[]{:S(2)}) collective-permute-start(f32[2,1536]{1,0:T(2,128)S(1)} %slice.101), channel_id=1, source_target_pairs={{1,0},{2,1},{3,2},{5,4},{6,5},{7,6},{9,8},{10,9},{11,10},{13,12},{... | collective-permute-start | bytes 36872 | tf_op jit(solution)/shard_map/ppermute | solution.py:10
  109.9 42.9 %all-gather.7.cloned.1.call-start = ((), (), s32[]{:S(2)}) async-start(), calls=%async_computation.4 | async-start | bytes 1966080 | tf_op jit(solution)/shard_map/all_gather | solution.py:90
  110.8 4.8 %collective-permute-start.2 = (f32[2,1536]{1,0:T(2,128)S(1)}, f32[2,1536]{1,0:T(2,128)S(1)}, u32[]{:S(2)}, u32[]{:S(2)}) collective-permute-start(f32[2,1536]{1,0:T(2,128)S(1)} %slice.98), channel_id=1, source_target_pairs={{1,0},{2,1},{3,2},{5,4},{6,5},{7,6},{9,8},{10,9},{11,10},{13,12},{... | collective-permute-start | bytes 36872 | tf_op jit(solution)/shard_map/ppermute | solution.py:10
  118.5 79.3 %all-gather.11.cloned.1.call-start = ((), (), s32[]{:S(2)}) async-start(), calls=%async_computation.7 | async-start | bytes 1966080 | tf_op jit(solution)/shard_map/all_gather | solution.py:92
  121.1 130.2 %reduce-scatter.2.cloned.1.call-start = ((), (), s32[]{:S(2)}) async-start(), calls=%async_computation.6 | async-start | bytes 2359296 | tf_op jit(solution)/shard_map/reduce_scatter | solution.py:107
  154.3 1.9 copy-start.8
  154.3 2.4 copy-start.17
  159.8 1.3 copy-start.5
  183.6 1.8 copy-start.7
  191.1 6.7 %copy-start.9 = (bf16[4,128,1024]{2,1,0:T(8,128)(2,1)S(1)}, bf16[4,128,1024]{2,1,0:T(8,128)(2,1)}, u32[]{:S(2)}) copy-start(bf16[4,128,1024]{2,1,0:T(8,128)(2,1)} %copy.37) | copy-start | bytes 3145732
  203.8 52.5 %copy-start.6 = (bf16[512,1536]{1,0:T(8,128)(2,1)S(1)}, bf16[512,1536]{1,0:T(8,128)(2,1)}, u32[]{:S(2)}) copy-start(bf16[512,1536]{1,0:T(8,128)(2,1)} %all-gather.7.cloned.1.call-done) | copy-start | bytes 4718596
  222.4 39.5 %copy-start.14 = (f32[3,1536]{1,0:T(4,128)}, f32[3,1536]{1,0:T(4,128)S(1)}, u32[]{:S(2)}) copy-start(f32[3,1536]{1,0:T(4,128)S(1)} %get-tuple-element.65) | copy-start | bytes 55300
  222.4 39.5 %copy-start.15 = (f32[3,1536]{1,0:T(4,128)}, f32[3,1536]{1,0:T(4,128)S(1)}, u32[]{:S(2)}) copy-start(f32[3,1536]{1,0:T(4,128)S(1)} %get-tuple-element.66) | copy-start | bytes 55300
  252.9 35.9 %all-to-all-start = ((bf16[4,16,1024]{2,1,0:T(8,128)(2,1)}), bf16[4,16,1024]{2,1,0:T(8,128)(2,1)S(1)}, u32[]{:S(2)}, u32[]{:S(2)}) async-start(bf16[4,16,1024]{2,1,0:T(8,128)(2,1)} %bitcast.6), calls=%async_computation.1 | async-start | bytes 262144 | tf_op jit(solution)/shard_map/all_to_all | solution.py:114
  262.0 27.5 %copy-start.1 = (bf16[1024,1536]{1,0:T(8,128)(2,1)S(1)}, bf16[1024,1536]{1,0:T(8,128)(2,1)}, u32[]{:S(2)}) copy-start(bf16[1024,1536]{1,0:T(8,128)(2,1)} %param.15) | copy-start | bytes 9437188
Sparse Core Ops, SparseCore 0:
  9.6 84.7 all-gather.4
  110.0 21.4 all-gather.8
  133.1 19.6 all-gather.6
  154.2 24.6 all-gather.10
  182.2 68.9 reduce-scatter.1
where the time goes:
time: 297 us; the launch traced here: 296 us
  waiting for transfers between devices  136 us (46%)
  blocking collectives  53.9 us (18%)
  matrix products  31.7 us (11%)
  local copies, waits for them, and re-layouts  31 us (10%)
  other arithmetic  16.2 us (5%)
  between operations  14.1 us (5%)
  starting transfers between devices  13 us (4%)
    all_gather x1, waiting for transfers between devices, per_device(): down_whole = lax.all_gather(w_down, 'tp', axis=1, tiled=True)  72.5 us
    reduce_scatter x1, waiting for transfers between devices, per_device(): lax.psum_scatter(contract_last(select_rows(all_up_act), w_act) + contract...  28.7 us
    unnamed x40, local copies, waits for them, and re-layouts  23.3 us
    all_to_all x1, blocking collectives, per_device(): lax.all_to_all(cotangent, 'tp', split_axis=1, concat_axis=0, tiled=True)  21.8 us
    psum x1, blocking collectives, per_device(): lax.psum((jnp.sum(grad_w_act * grad_w_act, axis=1), jnp.sum(grad_w_val *...  20.2 us
    all_gather x1, waiting for transfers between devices, per_device(): lax.all_gather(grad_up_act, 'tp', axis=0, tiled=True)  18.6 us
    dot_general x3, matrix products, contract_first(): lax.dot_general(left, right, (((0,), (0,)), ((), ())), preferred_element_...  17.5 us
    dot_general x3, matrix products, contract_last(): lax.dot_general(left, right, (((1,), (1,)), ((), ())), preferred_element_...  14.3 us
  transfers between devices with their start and end apart: 10, of which 6 were waited for; matrix products, arithmetic and copies ran while one was open for 21% of the time, Pallas kernels for 0%

commit v1 on v0

--- a/solution.py
+++ b/solution.py
@@ -2,6 +2,17 @@
 import jax.numpy as jnp
 from jax import lax
 from jax.sharding import PartitionSpec as P
+
+
+def turned_line(block, axis, dim):
+    count = lax.axis_size(axis)
+    forward = [(i, (i + 1) % count) for i in range(count)]
+    parts = [block]
+    for far in range(1, count):
+        parts = [lax.ppermute(parts[0], axis, forward), *parts]
+    whole = jnp.concatenate(parts, axis=dim)
+    turn = (lax.axis_index(axis) + 1) * parts[-1].shape[dim]
+    return jnp.roll(whole, turn, axis=dim)
 
 
 def passed_along(value, axis, by):
@@ -67,7 +78,7 @@
     reach = tap_count - 1
     tp_count = lax.axis_size("tp")
     fs_count = lax.axis_size("fs")
-    down_whole = lax.all_gather(w_down, "tp", axis=1, tiled=True)
+    down_whole = turned_line(w_down, "tp", 1)
     prev_act, prev_val = passed_along(
         (up_act[local_rows - reach :], up_val[local_rows - reach :]), "tp", 1
     )

time: 297 us -> 373 us (1.26)
  local copies, waits for them, and re-layouts: 31 us -> 71 us
  waiting for transfers between devices: 136 us -> 160 us
  other arithmetic: 16.2 us -> 31 us
    ppermute x0 -> x3, waiting for transfers between devices: none -> 91.3 us  [turned_line(): parts = [lax.ppermute(parts[0], axis, forward), *parts]]
    all_gather x1 -> x0, waiting for transfers between devices: 72.5 us -> none  [per_device(): down_whole = lax.all_gather(w_down, 'tp', axis=1, tiled=True)]
    unnamed x40 -> x63, local copies, waits for them, and re-layouts: 23.3 us -> 48.6 us
    reduce_sum x2, other arithmetic: 3.01 us -> 13.8 us  [tap_grads(): jnp.sum(grad_pre * extended[offset:offset + length], axis=0)]
    ppermute x4, waiting for transfers between devices: 5.15 us -> 13.6 us  [passed_along(): return lax.ppermute(value, axis, pairs)]
    all_gather x0 -> x2, local copies, waits for them, and re-layouts: none -> 5.15 us  [the longest x1 2.58 us: per_device(): lax.all_gather(grad_up_val, 'tp', axis=0, tiled=True)]
    reshape x2 -> x0, local copies, waits for them, and re-layouts: 4.18 us -> none  [select_rows(): shaped = gathered.reshape(tp_count, fs_count, shard_rows, gathered.shape[1])]
    transpose x0 -> x2, local copies, waits for them, and re-layouts: none -> 4.18 us  [select_rows(): jnp.transpose(shaped, (1, 0, 2, 3))]
  transfers between devices with their start and end apart: 10 -> 12, of which waited for: 6 -> 8; matrix products, arithmetic and copies ran while one was open for 21% -> 21% of each run, Pallas kernels for 0% -> 0%
where the time goes in v1:
time: 373 us; the launch traced here: 371 us
  waiting for transfers between devices  160 us (43%)
  local copies, waits for them, and re-layouts  71 us (19%)
  blocking collectives  52.7 us (14%)
  other arithmetic  31 us (8%)
  matrix products  28.9 us (8%)
  between operations  14.2 us (4%)
  starting transfers between devices  13.9 us (4%)
    ppermute x3, waiting for transfers between devices, turned_line(): parts = [lax.ppermute(parts[0], axis, forward), *parts]  91.3 us
    unnamed x63, local copies, waits for them, and re-layouts  48.6 us
    reduce_scatter x1, waiting for transfers between devices, per_device(): lax.psum_scatter(contract_last(select_rows(all_up_act), w_act) + contract...  28.9 us
    all_to_all x1, blocking collectives, per_device(): lax.all_to_all(cotangent, 'tp', split_axis=1, concat_axis=0, tiled=True)  20.5 us
    psum x1, blocking collectives, per_device(): lax.psum((jnp.sum(grad_w_act * grad_w_act, axis=1), jnp.sum(grad_w_val *...  20.2 us
    dot_general x3, matrix products, contract_first(): lax.dot_general(left, right, (((0,), (0,)), ((), ())), preferred_element_...  17.4 us
    all_gather x1, waiting for transfers between devices, per_device(): lax.all_gather(grad_up_act, 'tp', axis=0, tiled=True)  16.7 us
    reduce_sum x2, other arithmetic, tap_grads(): jnp.sum(grad_pre * extended[offset:offset + length], axis=0)  13.8 us
  transfers between devices with their start and end apart: 12, of which 8 were waited for; matrix products, arithmetic and copies ran while one was open for 21% of the time, Pallas kernels for 0%

profile of v1, /device:TPU:0, one launch (start us, length us, event | category | flops | bytes accessed | tf_op | source)
XLA Modules:
  0.0 371.3 jit_solution(12499299515752738530)
XLA Ops:
  7.8 37.1 %collective-permute-done = bf16[1536,1024]{1,0:T(8,128)(2,1)S(1)} collective-permute-done((bf16[1536,1024]{1,0:T(8,128)(2,1)}, bf16[1536,1024]{1,0:T(8,128)(2,1)S(1)}, u32[]{:S(2)}, u32[]{:S(2)}) %collective-permute-start) | collective-permute-done | bytes 3145760 | tf_op jit(solution)/shard_map/ppermute | solution.py:12
  46.6 36.8 %collective-permute-done.1 = bf16[1536,1024]{1,0:T(8,128)(2,1)} collective-permute-done((bf16[1536,1024]{1,0:T(8,128)(2,1)S(1)}, bf16[1536,1024]{1,0:T(8,128)(2,1)}, u32[]{:S(2)}, u32[]{:S(2)}) %collective-permute-start.1) | collective-permute-done | bytes 3145760 | tf_op jit(solution)/shard_map/ppermute | solution.py:12
  85.0 5.1 %collective-permute-start.3 = (bf16[2,1536]{0,1:T(8,128)(2,1)}, bf16[2,1536]{0,1:T(8,128)(2,1)}, u32[]{:S(2)}, u32[]{:S(2)}) collective-permute-start(bf16[2,1536]{0,1:T(8,128)(2,1)} %copy.57), channel_id=1, source_target_pairs={{0,1},{1,2},{2,3},{4,5},{5,6},{6,7},{8,9},{9,10},{10,11},{12,13},{... | collective-permute-start | bytes 18440 | tf_op jit(solution)/shard_map/ppermute | solution.py:21
  102.8 17.5 %collective-permute-done.2 = bf16[1536,1024]{1,0:T(8,128)(2,1)} collective-permute-done((bf16[1536,1024]{1,0:T(8,128)(2,1)}, bf16[1536,1024]{1,0:T(8,128)(2,1)}, u32[]{:S(2)}, u32[]{:S(2)}) %collective-permute-start.2) | collective-permute-done | bytes 3145760 | tf_op jit(solution)/shard_map/ppermute | solution.py:12
  120.3 3.9 %constant_dynamic-update-slice_fusion.7 = bf16[1536,8192]{1,0:T(8,128)(2,1)} fusion(bf16[1536,1024]{1,0:T(8,128)(2,1)} %collective-permute-done.2), kind=kLoop, calls=%fused_computation.61 | loop fusion | bytes 6291456
  124.2 4.0 %constant_dynamic-update-slice_fusion.6 = bf16[1536,8192]{1,0:T(8,128)(2,1)} fusion(bf16[1536,8192]{1,0:T(8,128)(2,1)} %constant_dynamic-update-slice_fusion.7, bf16[1536,1024]{1,0:T(8,128)(2,1)} %collective-permute-done.1), kind=kLoop, calls=%fused_computation.60 | loop fusion | bytes 6291456
  133.2 3.8 %constant_dynamic-update-slice_fusion.3 = bf16[1536,8192]{1,0:T(8,128)(2,1)} fusion(bf16[1536,8192]{1,0:T(8,128)(2,1)} %constant_dynamic-update-slice_fusion.4, bf16[1536,1024]{1,0:T(8,128)(2,1)} %collective-permute-done.2), kind=kLoop, calls=%fused_computation.57 | loop fusion | bytes 6291456
  137.0 3.8 %constant_dynamic-update-slice_fusion.2 = bf16[1536,8192]{1,0:T(8,128)(2,1)} fusion(bf16[1536,8192]{1,0:T(8,128)(2,1)} %constant_dynamic-update-slice_fusion.3, bf16[1536,1024]{1,0:T(8,128)(2,1)} %collective-permute-done.1), kind=kLoop, calls=%fused_computation.56 | loop fusion | bytes 6291456
  144.7 6.5 %fusion.5 = bf16[128,1536]{0,1:T(8,128)(2,1)S(1)} fusion(bf16[128,4096]{1,0:T(8,128)(2,1)S(1)} %copy-done.10, bf16[1536,8192]{1,0:T(8,128)(2,1)} %constant_dynamic-update-slice_fusion, s32[]{:T(128)S(6)} %select_n.14), kind=kOutput, calls=%fused_computation.8 | convolution fusion | flops 1610809344 | bytes 14024708 | tf_op jit(solution)/shard_map/dot_general | solution.py:25
  151.3 4.1 %multiply_reduce_fusion.5 = (f32[1536]{0:T(1024)}, f32[1536]{0:T(1024)}, f32[1536]{0:T(1024)}, f32[1536]{0:T(1024)}, f32[128,1536]{0,1:T(8,128)}, /*index=5*/f32[128,1536]{0,1:T(8,128)}) fusion(f32[130,1536]{0,1:T(8,128)S(1)} %maximum_convert_fusion, bf16[128,1536]{0,1:T(8,128)(2,1)S(1)} %fusion.5, f32[130,1536]{0,1:T(8,128)S(1)} %maximum_convert_fusion.1, ...), kind=kLoop, calls=%fused_computation.42 | loop fusion | flops 4515840 | bytes 6733824 | tf_op jit(solution)/shard_map/reduce_sum | solution.py:57
  161.4 9.1 %collective-permute-done.6 = f32[2,1536]{1,0:T(2,128)} collective-permute-done((f32[2,1536]{1,0:T(2,128)}, f32[2,1536]{1,0:T(2,128)}, u32[]{:S(2)}, u32[]{:S(2)}) %collective-permute-start.6) | collective-permute-done | bytes 12320 | tf_op jit(solution)/shard_map/ppermute | solution.py:21
  172.4 9.6 %multiply_reduce_fusion.8 = (f32[1536]{0:T(1024)}, f32[1536]{0:T(1024)}, f32[1536]{0:T(1024)}, f32[1536]{0:T(1024)}, f32[128,1536]{0,1:T(8,128)}, /*index=5*/f32[128,1536]{0,1:T(8,128)}, bf16[128,1536]{0,1:T(8,128)(2,1)}) fusion(f32[130,1536]{0,1:T(8,128)} %copy-done.3, f32[128,1536]{0,1:T(8,128)} %get-tuple-element.83, bf16[128,1536]{0,1:T(8,128)(2,1)S(1)} %fusion.5, ...), kind=kLoop, calls=%fused_computation.45 | loop fusion | flops 8251392 | bytes 8712192 | tf_op jit(solution)/shard_map/reduce_sum | solution.py:57
  184.8 4.4 %collective-permute-done.5 = f32[2,1536]{1,0:T(2,128)S(1)} collective-permute-done((f32[2,1536]{1,0:T(2,128)S(1)}, f32[2,1536]{1,0:T(2,128)S(1)}, u32[]{:S(2)}, u32[]{:S(2)}) %collective-permute-start.5) | collective-permute-done | bytes 12320 | tf_op jit(solution)/shard_map/ppermute | solution.py:21
  190.5 4.4 %fusion.23 = bf16[128,1536]{0,1:T(8,128)(2,1)} fusion(f32[128,1536]{0,1:T(8,128)} %get-tuple-element.84, f32[2,1536]{0,1:T(8,128)} %copy.62, f32[1536]{0:T(1024)S(1)} %get-tuple-element.72, f32[1536]{0:T(1024)} %get-tuple-element.73, f32[1536]{0:T(1024)S(1)} %get-tuple-element.71), kind=kLoop, calls=%fused_computation.33 | loop fusion | flops 1572864 | bytes 1210368 | tf_op jit(solution)/shard_map/convert_element_type | solution.py:51
  194.9 2.4 multiply_convert_fusion
  197.6 9.1 %all-gather.6.cloned.1.call-done = bf16[512,1536]{0,1:T(8,128)(2,1)} async-done(((bf16[128,1536]{0,1:T(8,128)(2,1)}), bf16[512,1536]{0,1:T(8,128)(2,1)}) %all-gather.6.cloned.1.call-update) | async-done | bytes 1572880 | tf_op jit(solution)/shard_map/all_gather | solution.py:102
  206.7 2.6 copy.67
  209.3 2.7 copy.68
  212.0 16.7 %all-gather.4.cloned.1.call-done = bf16[512,1536]{0,1:T(8,128)(2,1)} async-done(((bf16[128,1536]{0,1:T(8,128)(2,1)}), bf16[512,1536]{0,1:T(8,128)(2,1)}) %all-gather.4.cloned.1.call-update) | async-done | bytes 1572880 | tf_op jit(solution)/shard_map/all_gather | solution.py:101
  228.7 2.6 copy.63
  235.2 3.2 convolution_add_fusion
  239.1 20.5 %all_to_all.38 = bf16[128,4,1024]{0,2,1:T(8,128)(2,1)S(1)} all-to-all(bf16[128,4,1024]{0,2,1:T(8,128)(2,1)S(1)} %bitcast.41), channel_id=1, replica_groups=mesh['fs'=8,'tp'=4] {'tp'}, dimensions={1} | all-to-all | bytes 2097152 | tf_op jit(solution)/shard_map/all_to_all | solution.py:105
  260.4 6.0 %multiply_reduce_fusion = (f32[1536]{0:T(1024)S(1)}, f32[1536,1024]{0,1:T(8,128)}) fusion(bf16[512,1536]{0,1:T(8,128)(2,1)} %all-gather.8.cloned.1.call-done, bf16[512,1024]{1,0:T(8,128)(2,1)S(1)} %bitcast.44), kind=kOutput, calls=%fused_computation.2 | convolution fusion | flops 1613756928 | bytes 8919040 | tf_op jit(solution)/shard_map/dot_general | solution.py:31
  266.4 6.7 %copy.74 = f32[1536,1024]{1,0:T(8,128)} copy(f32[1536,1024]{0,1:T(8,128)} %get-tuple-element.88) | data formatting | bytes 12582912
  273.0 5.7 %multiply_reduce_fusion.1 = (f32[1024]{0:T(1024)S(1)}, f32[1024,1536]{0,1:T(8,128)}) fusion(bf16[512,1536]{0,1:T(8,128)(2,1)S(1)} %copy-done.8, bf16[512,1024]{1,0:T(8,128)(2,1)} %param.11), kind=kOutput, calls=%fused_computation.3 | convolution fusion | flops 1613757440 | bytes 8916992 | tf_op jit(solution)/shard_map/dot_general | solution.py:31
  278.8 6.7 %copy.73 = f32[1024,1536]{1,0:T(8,128)} copy(f32[1024,1536]{0,1:T(8,128)} %get-tuple-element.92) | data formatting | bytes 12582912
  285.5 12.0 %all-reduce.1 = (f32[3,1536]{1,0:T(4,128)S(1)}, f32[3,1536]{1,0:T(4,128)S(1)}, f32[1536]{0:T(1024)}, f32[1536]{0:T(1024)}, f32[1536]{0:T(1024)}) all-reduce(f32[3,1536]{1,0:T(4,128)S(1)} %pad_maximum_fusion.2, f32[3,1536]{1,0:T(4,128)S(1)} %pad_maximum_fusion.3, f32[1536]{0:T(1024)S(1)} %copy-done.14, ...), channel_id=1, replica_groups=mesh['fs'=8,'tp'=4] {'tp'}, use_global_device_ids=true, to_apply=%region_4.5 | all-reduce | flops 13824 | bytes 110592 | tf_op jit(solution)/shard_map/psum | solution.py:127
  297.7 28.9 %reduce-scatter.2.cloned.1.call-done = f32[64,1024]{1,0:T(8,128)} async-done(((f32[512,1024]{1,0:T(8,128)}), f32[64,1024]{1,0:T(8,128)}) %reduce-scatter.2.cloned.1.call-update) | async-done | bytes 262160 | tf_op jit(solution)/shard_map/reduce_scatter | solution.py:118
  328.2 3.3 all-to-all-start
  331.5 5.7 %multiply_reduce_fusion.2 = (f32[1024]{0:T(1024)S(1)}, f32[1024,1536]{0,1:T(8,128)}) fusion(bf16[512,1536]{0,1:T(8,128)(2,1)S(1)} %copy-done.7, bf16[512,1024]{1,0:T(8,128)(2,1)} %param.11), kind=kOutput, calls=%fused_computation.4 | convolution fusion | flops 1613757440 | bytes 8916992 | tf_op jit(solution)/shard_map/dot_general | solution.py:31
  337.2 6.7 %copy.72 = f32[1024,1536]{1,0:T(8,128)} copy(f32[1024,1536]{0,1:T(8,128)} %get-tuple-element.90) | data formatting | bytes 12582912
  343.9 20.2 %all-reduce = (f32[1024]{0:T(1024)}, f32[1024]{0:T(1024)}, f32[2,3]{1,0:T(2,128)}) all-reduce(f32[1024]{0:T(1024)S(1)} %get-tuple-element.89, f32[1024]{0:T(1024)S(1)} %get-tuple-element.91, f32[2,3]{1,0:T(2,128)S(1)} %pad_maximum_fusion.4), channel_id=1, replica_groups=mesh['fs'=8,'tp'=4] {'fs'}, use_global_device_ids=true, to_apply=%region_14.15 | all-reduce | flops 2054 | bytes 16432 | tf_op jit(solution)/shard_map/psum | solution.py:133
  (104 shorter events, 45.3 us)
Async XLA Ops:
  7.2 225.6 %copy-start = (bf16[1024,1536]{1,0:T(8,128)(2,1)S(1)}, bf16[1024,1536]{1,0:T(8,128)(2,1)}, u32[]{:S(2)}) copy-start(bf16[1024,1536]{1,0:T(8,128)(2,1)} %param.15) | copy-start | bytes 9437188
  7.2 199.5 %all-gather.6.cloned.1.call-start = ((), (), s32[]{:S(2)}) async-start(), calls=%async_computation.4 | async-start | bytes 1966080 | tf_op jit(solution)/shard_map/all_gather | solution.py:102
  7.2 37.6 %collective-permute-start = (bf16[1536,1024]{1,0:T(8,128)(2,1)}, bf16[1536,1024]{1,0:T(8,128)(2,1)S(1)}, u32[]{:S(2)}, u32[]{:S(2)}) collective-permute-start(bf16[1536,1024]{1,0:T(8,128)(2,1)} %param.17), channel_id=1, source_target_pairs={{0,1},{1,2},{2,3},{3,0},{4,5},{5,6},{6,7},{7,4},{8,9},{9,10},{10,1... | collective-permute-start | bytes 9437192 | tf_op jit(solution)/shard_map/ppermute | solution.py:12
  46.5 36.8 %collective-permute-start.1 = (bf16[1536,1024]{1,0:T(8,128)(2,1)S(1)}, bf16[1536,1024]{1,0:T(8,128)(2,1)}, u32[]{:S(2)}, u32[]{:S(2)}) collective-permute-start(bf16[1536,1024]{1,0:T(8,128)(2,1)S(1)} %collective-permute-done), channel_id=1, source_target_pairs={{0,1},{1,2},{2,3},{3,0},{4,5},{5,6},{6,7},{7,4},{8,9},{9,10},{10,1... | collective-permute-start | bytes 9437192 | tf_op jit(solution)/shard_map/ppermute | solution.py:12
  83.3 37.0 %collective-permute-start.2 = (bf16[1536,1024]{1,0:T(8,128)(2,1)}, bf16[1536,1024]{1,0:T(8,128)(2,1)}, u32[]{:S(2)}, u32[]{:S(2)}) collective-permute-start(bf16[1536,1024]{1,0:T(8,128)(2,1)} %collective-permute-done.1), channel_id=1, source_target_pairs={{0,1},{1,2},{2,3},{3,0},{4,5},{5,6},{6,7},{7,4},{8,9},{9,10},{10,1... | collective-permute-start | bytes 9437192 | tf_op jit(solution)/shard_map/ppermute | solution.py:12
  85.0 14.7 %collective-permute-start.3 = (bf16[2,1536]{0,1:T(8,128)(2,1)}, bf16[2,1536]{0,1:T(8,128)(2,1)}, u32[]{:S(2)}, u32[]{:S(2)}) collective-permute-start(bf16[2,1536]{0,1:T(8,128)(2,1)} %copy.57), channel_id=1, source_target_pairs={{0,1},{1,2},{2,3},{4,5},{5,6},{6,7},{8,9},{9,10},{10,11},{12,13},{... | collective-permute-start | bytes 18440 | tf_op jit(solution)/shard_map/ppermute | solution.py:21
  91.8 9.4 %collective-permute-start.4 = (bf16[2,1536]{0,1:T(8,128)(2,1)}, bf16[2,1536]{0,1:T(8,128)(2,1)}, u32[]{:S(2)}, u32[]{:S(2)}) collective-permute-start(bf16[2,1536]{0,1:T(8,128)(2,1)} %copy.59), channel_id=1, source_target_pairs={{0,1},{1,2},{2,3},{4,5},{5,6},{6,7},{8,9},{9,10},{10,11},{12,13},{... | collective-permute-start | bytes 18440 | tf_op jit(solution)/shard_map/ppermute | solution.py:21
  101.2 50.0 %copy-start.2 = (f32[130,1536]{0,1:T(8,128)}, f32[130,1536]{0,1:T(8,128)S(1)}, u32[]{:S(2)}) copy-start(f32[130,1536]{0,1:T(8,128)S(1)} %maximum_convert_fusion) | copy-start | bytes 2396164
  102.8 48.4 %copy-start.3 = (f32[130,1536]{0,1:T(8,128)}, f32[130,1536]{0,1:T(8,128)S(1)}, u32[]{:S(2)}) copy-start(f32[130,1536]{0,1:T(8,128)S(1)} %maximum_convert_fusion.1) | copy-start | bytes 2396164
  124.2 4.1 %copy-start.6 = (bf16[1536,1024]{1,0:T(8,128)(2,1)S(1)}, bf16[1536,1024]{1,0:T(8,128)(2,1)}, u32[]{:S(2)}) copy-start(bf16[1536,1024]{1,0:T(8,128)(2,1)} %copy-done.5) | copy-start | bytes 9437188
  144.7 6.5 %copy-start.12 = (f32[1536]{0:T(1024)S(1)}, f32[1536]{0:T(1024)}, u32[]{:S(2)}) copy-start(f32[1536]{0:T(1024)} %get-tuple-element.73) | copy-start | bytes 18436
  144.7 6.5 %copy-start.21 = (f32[1536]{0:T(1024)S(1)}, f32[1536]{0:T(1024)}, u32[]{:S(2)}) copy-start(f32[1536]{0:T(1024)} %convert_element_type.56) | copy-start | bytes 18436
  157.4 13.2 %collective-permute-start.6 = (f32[2,1536]{1,0:T(2,128)}, f32[2,1536]{1,0:T(2,128)}, u32[]{:S(2)}, u32[]{:S(2)}) collective-permute-start(f32[2,1536]{1,0:T(2,128)} %copy.65), channel_id=1, source_target_pairs={{1,0},{2,1},{3,2},{5,4},{6,5},{7,6},{9,8},{10,9},{11,10},{13,12},{... | collective-permute-start | bytes 36872 | tf_op jit(solution)/shard_map/ppermute | solution.py:21
  182.1 46.6 %all-gather.4.cloned.1.call-start = ((), (), s32[]{:S(2)}) async-start(), calls=%async_computation.3 | async-start | bytes 1966080 | tf_op jit(solution)/shard_map/all_gather | solution.py:101
  183.5 5.7 %collective-permute-start.5 = (f32[2,1536]{1,0:T(2,128)S(1)}, f32[2,1536]{1,0:T(2,128)S(1)}, u32[]{:S(2)}, u32[]{:S(2)}) collective-permute-start(f32[2,1536]{1,0:T(2,128)S(1)} %copy.61), channel_id=1, source_target_pairs={{1,0},{2,1},{3,2},{5,4},{6,5},{7,6},{9,8},{10,9},{11,10},{13,12},{... | collective-permute-start | bytes 36872 | tf_op jit(solution)/shard_map/ppermute | solution.py:21
  194.9 65.5 %all-gather.8.cloned.1.call-start = ((), (), s32[]{:S(2)}) async-start(), calls=%async_computation.6 | async-start | bytes 1966080 | tf_op jit(solution)/shard_map/all_gather | solution.py:103
  197.4 129.1 %reduce-scatter.2.cloned.1.call-start = ((), (), s32[]{:S(2)}) async-start(), calls=%async_computation.5 | async-start | bytes 2359296 | tf_op jit(solution)/shard_map/reduce_scatter | solution.py:118
  235.2 3.2 copy-start.11
  238.4 21.8 %copy-start.17 = (f32[1536]{0:T(1024)S(1)}, f32[1536]{0:T(1024)}, u32[]{:S(2)}) copy-start(f32[1536]{0:T(1024)} %get-tuple-element.60) | copy-start | bytes 18436
  238.4 21.8 %copy-start.16 = (f32[1536]{0:T(1024)S(1)}, f32[1536]{0:T(1024)}, u32[]{:S(2)}) copy-start(f32[1536]{0:T(1024)} %get-tuple-element.62) | copy-start | bytes 18436
  238.4 21.8 %copy-start.15 = (f32[1536]{0:T(1024)S(1)}, f32[1536]{0:T(1024)}, u32[]{:S(2)}) copy-start(f32[1536]{0:T(1024)} %get-tuple-element.61) | copy-start | bytes 18436
  238.4 21.9 %copy-start.20 = (f32[1536]{0:T(1024)S(1)}, f32[1536]{0:T(1024)}, u32[]{:S(2)}) copy-start(f32[1536]{0:T(1024)} %get-tuple-element.63) | copy-start | bytes 18436
  238.4 21.9 %copy-start.19 = (f32[1536]{0:T(1024)S(1)}, f32[1536]{0:T(1024)}, u32[]{:S(2)}) copy-start(f32[1536]{0:T(1024)} %get-tuple-element.65) | copy-start | bytes 18436
  238.4 21.9 %copy-start.18 = (f32[1536]{0:T(1024)S(1)}, f32[1536]{0:T(1024)}, u32[]{:S(2)}) copy-start(f32[1536]{0:T(1024)} %get-tuple-element.64) | copy-start | bytes 18436
  266.3 6.7 %copy-start.8 = (bf16[512,1536]{0,1:T(8,128)(2,1)S(1)}, bf16[512,1536]{0,1:T(8,128)(2,1)}, u32[]{:S(2)}) copy-start(bf16[512,1536]{0,1:T(8,128)(2,1)} %all-gather.6.cloned.1.call-done) | copy-start | bytes 4718596
  278.8 6.7 %copy-start.13 = (f32[1536]{0:T(1024)S(1)}, f32[1536]{0:T(1024)}, u32[]{:S(2)}) copy-start(f32[1536]{0:T(1024)} %get-tuple-element.66) | copy-start | bytes 18436
  278.8 6.7 %copy-start.14 = (f32[1536]{0:T(1024)S(1)}, f32[1536]{0:T(1024)}, u32[]{:S(2)}) copy-start(f32[1536]{0:T(1024)} %get-tuple-element.67) | copy-start | bytes 18436
  278.8 52.7 %copy-start.7 = (bf16[512,1536]{0,1:T(8,128)(2,1)S(1)}, bf16[512,1536]{0,1:T(8,128)(2,1)}, u32[]{:S(2)}) copy-start(bf16[512,1536]{0,1:T(8,128)(2,1)} %all-gather.4.cloned.1.call-done) | copy-start | bytes 4718596
  297.5 39.7 %copy-start.22 = (f32[3,1536]{1,0:T(4,128)}, f32[3,1536]{1,0:T(4,128)S(1)}, u32[]{:S(2)}) copy-start(f32[3,1536]{1,0:T(4,128)S(1)} %get-tuple-element.77) | copy-start | bytes 55300
  297.5 39.7 %copy-start.23 = (f32[3,1536]{1,0:T(4,128)}, f32[3,1536]{1,0:T(4,128)S(1)}, u32[]{:S(2)}) copy-start(f32[3,1536]{1,0:T(4,128)S(1)} %get-tuple-element.78) | copy-start | bytes 55300
  328.2 35.9 %all-to-all-start = ((bf16[4,16,1024]{2,1,0:T(8,128)(2,1)}), bf16[4,16,1024]{2,1,0:T(8,128)(2,1)S(1)}, u32[]{:S(2)}, u32[]{:S(2)}) async-start(bf16[4,16,1024]{2,1,0:T(8,128)(2,1)} %bitcast.7), calls=%async_computation.1 | async-start | bytes 262144 | tf_op jit(solution)/shard_map/all_to_all | solution.py:125
  337.2 27.6 %copy-start.1 = (bf16[1024,1536]{1,0:T(8,128)(2,1)S(1)}, bf16[1024,1536]{1,0:T(8,128)(2,1)}, u32[]{:S(2)}) copy-start(bf16[1024,1536]{1,0:T(8,128)(2,1)} %param.15) | copy-start | bytes 9437188
  (5 other events, 10.8 us)
Sparse Core Ops, SparseCore 0:
  182.2 24.4 all-gather.5
  208.8 19.8 all-gather.3
  230.2 23.5 all-gather.7
  257.2 69.3 reduce-scatter.1
